TPU v7x, 32 devices: a whole 2x2x4 slice. The times are simulated.
32 devices in a mesh: rep: 4 (over z), fs: 2 (over y), tp: 4 (over x, core).
Axes of the slice: x: 2, y: 2, z: 4, core: 2. Of those that a mesh axis runs over, the one named last changes fastest.
Arguments:
- inputs: bfloat16 [512, 4096], P('rep'), may hold values from -6 to 6
- cotangent: bfloat16 [512, 4096], P('rep'), may hold values from -6 to 6
- w_gate: bfloat16 [4096, 11264], P(None, ('fs', 'tp')), may hold values from -0.09375 to 0.09375
- w_upward: bfloat16 [4096, 11264], P(None, ('fs', 'tp')), may hold values from -0.09375 to 0.09375
- w_down: bfloat16 [11264, 4096], P(('fs', 'tp')), may hold values from -0.0546875 to 0.0546875
Outputs:
- grad_input: bfloat16 [512, 4096], P('rep')
- grad_gate: float32 [4096, 11264], P('rep', ('fs', 'tp'))
- grad_upward: float32 [4096, 11264], P('rep', ('fs', 'tp'))
- grad_down: float32 [11264, 4096], P(('fs', 'tp'), 'rep')
All inputs are finite; a program needn't handle non-finite values.
Results may differ from a plain program's by a relative error of at most 0.0049.
Values may be sent and summed in bfloat16 or wider, within the bound.
A program may use at most 128 MiB of HBM per device.

v0:
```python
import jax
import jax.numpy as jnp
from jax import lax
from jax.sharding import PartitionSpec as P


def contract_rows(left, right):
    return lax.dot_general(
        left, right, (((0,), (0,)), ((), ())), preferred_element_type=jnp.float32
    )


def contract_cols(left, right):
    return lax.dot_general(
        left, right, (((1,), (1,)), ((), ())), preferred_element_type=jnp.float32
    )


def local(inputs, cotangent, w_gate, w_upward, w_down):
    gate_pre = jnp.dot(inputs, w_gate, preferred_element_type=jnp.float32)
    up_pre = jnp.dot(inputs, w_upward, preferred_element_type=jnp.float32)
    sigmoid_gate = jax.nn.sigmoid(gate_pre)
    activated = gate_pre * sigmoid_gate
    hidden = (activated * up_pre).astype(jnp.bfloat16)
    hidden_grad = contract_cols(cotangent, w_down)
    gate_delta = (
        hidden_grad * up_pre * sigmoid_gate * (1.0 + gate_pre * (1.0 - sigmoid_gate))
    ).astype(jnp.bfloat16)
    up_delta = (hidden_grad * activated).astype(jnp.bfloat16)
    input_cols, cotangent_cols = (
        lax.all_to_all(inputs, "rep", split_axis=1, concat_axis=0, tiled=True),
        lax.all_to_all(cotangent, "rep", split_axis=1, concat_axis=0, tiled=True),
    )
    piece_gate = lax.all_gather(gate_delta, "rep", axis=0, tiled=True)
    piece_up = lax.all_gather(up_delta, "rep", axis=0, tiled=True)
    piece_hidden = lax.all_gather(hidden, "rep", axis=0, tiled=True)
    grad_gate = contract_rows(input_cols, piece_gate)
    grad_upward = contract_rows(input_cols, piece_up)
    grad_down = contract_rows(piece_hidden, cotangent_cols)
    input_terms = contract_cols(gate_delta, w_gate) + contract_cols(up_delta, w_upward)
    grad_input = lax.psum(input_terms, ("fs", "tp")).astype(jnp.bfloat16)
    return (grad_input, grad_gate, grad_upward, grad_down)


def solution(mesh):
    in_specs = (
        P("rep", None),
        P("rep", None),
        P(None, ("fs", "tp")),
        P(None, ("fs", "tp")),
        P(("fs", "tp"), None),
    )
    out_specs = (
        P("rep", None),
        P("rep", ("fs", "tp")),
        P("rep", ("fs", "tp")),
        P(("fs", "tp"), "rep"),
    )
    return jax.shard_map(local, mesh=mesh, in_specs=in_specs, out_specs=out_specs, check_vma=False)
```

profile of v0, /device:TPU:0, one launch (start us, length us, event | category | flops | bytes accessed | tf_op | source)
XLA Modules:
  0.0 190.2 jit_solution(5874101361756558968)
XLA Ops:
  7.2 0.0 copy-start.2
  7.2 0.0 all-gather.4.cloned.1.call-start
  7.2 0.0 copy-start
  7.2 8.6 %fusion.1 = f32[128,1408]{1,0:T(8,128)S(1)} fusion(bf16[128,4096]{1,0:T(8,128)(2,1)} %param.6, bf16[1408,4096]{1,0:T(8,128)(2,1)} %param.9), kind=kOutput, calls=%fused_computation.8 | convolution fusion | flops 1476395008 | bytes 13303808 | tf_op jit(solution)/shard_map/dot_general | solution.py:14
  15.8 0.0 copy-done.2
  15.8 0.0 copy-done
  15.8 0.0 copy-start.1
  15.8 1.8 fusion.2
  17.7 2.4 %copy-done.1 = bf16[4096,1408]{1,0:T(8,128)(2,1)S(1)} copy-done((bf16[4096,1408]{1,0:T(8,128)(2,1)S(1)}, bf16[4096,1408]{1,0:T(8,128)(2,1)}, u32[]{:S(2)}) %copy-start.1) | copy-done | bytes 11534360
  20.1 3.0 %multiply_convert_fusion = (bf16[128,1408]{1,0:T(8,128)(2,1)}, bf16[128,1408]{1,0:T(8,128)(2,1)}, bf16[128,1408]{1,0:T(8,128)(2,1)}) fusion(f32[128,1408]{1,0:T(8,128)S(1)} %fusion.2, f32[128,1408]{1,0:T(8,128)S(1)} %fusion.1, bf16[128,4096]{1,0:T(8,128)(2,1)S(1)} %copy-done.2, bf16[4096,1408]{1,0:T(8,128)(2,1)S(1)} %copy-done.1), kind=kOutput, calls=%fused_computation.3 | convolution fusion | flops 1479098368 | bytes 15106048 | tf_op jit(solution)/shard_map/dot_general | solution.py:21
  23.1 0.0 copy-start.3
  23.1 0.0 copy-start.4
  23.1 0.0 all-gather.4.cloned.1.call-update
  23.1 0.0 all-gather.6.cloned.1.call-start
  23.2 0.7 all-gather.6.cloned.1.call-update
  23.9 1.3 copy.13
  25.2 6.3 %all-to-all-start = ((bf16[128,4,1024]{0,2,1:T(8,128)(2,1)}), bf16[128,4,1024]{0,2,1:T(8,128)(2,1)S(1)}, u32[]{:S(2)}, u32[]{:S(2)}) async-start(bf16[128,4,1024]{0,2,1:T(8,128)(2,1)} %bitcast.27), calls=%async_computation | async-start | bytes 2097152 | tf_op jit(solution)/shard_map/all_to_all | solution.py:31
  31.5 0.0 all-gather.8.cloned.1.call-start
  31.5 0.7 all-gather.8.cloned.1.call-update
  32.3 0.0 copy-done.3
  32.3 1.3 copy.15
  33.6 0.0 copy-done.4
  33.6 9.5 %fusion.3 = f32[128,4096]{1,0:T(8,128)} fusion(bf16[128,1408]{1,0:T(8,128)(2,1)S(1)} %copy-done.4, bf16[4096,1408]{1,0:T(8,128)(2,1)} %param.7), kind=kOutput, calls=%fused_computation.10 | convolution fusion | flops 1476395008 | bytes 13991936 | tf_op jit(solution)/shard_map/dot_general | solution.py:14
  43.1 37.0 %all-to-all-done = bf16[128,4,1024]{0,2,1:T(8,128)(2,1)S(1)} async-done(((bf16[128,4,1024]{0,2,1:T(8,128)(2,1)}), bf16[128,4,1024]{0,2,1:T(8,128)(2,1)S(1)}, u32[]{:S(2)}, u32[]{:S(2)}) %all-to-all-start) | async-done | bytes 1048608 | tf_op jit(solution)/shard_map/all_to_all | solution.py:31
  80.1 4.3 %all-to-all-start.1 = ((bf16[128,4,1024]{0,2,1:T(8,128)(2,1)}), bf16[128,4,1024]{0,2,1:T(8,128)(2,1)}, u32[]{:S(2)}, u32[]{:S(2)}) async-start(bf16[128,4,1024]{0,2,1:T(8,128)(2,1)} %bitcast.5), calls=%async_computation.1 | async-start | bytes 2097152 | tf_op jit(solution)/shard_map/all_to_all | solution.py:32
  84.3 9.0 %convolution_add_fusion = f32[128,4096]{1,0:T(8,128)S(1)} fusion(f32[128,4096]{1,0:T(8,128)} %fusion.3, bf16[128,1408]{1,0:T(8,128)(2,1)} %get-tuple-element.18, bf16[4096,1408]{1,0:T(8,128)(2,1)} %param.8), kind=kOutput, calls=%fused_computation | convolution fusion | flops 1476919296 | bytes 16089088 | tf_op jit(solution)/shard_map/dot_general | solution.py:14
  93.3 59.1 %all-reduce.1 = bf16[128,4096]{1,0:T(8,128)(2,1)} all-reduce(f32[128,4096]{1,0:T(8,128)S(1)} %convolution_add_fusion), channel_id=1, replica_groups=mesh['rep'=4,'fs'=2,'tp'=4] {'fs','tp'}, use_global_device_ids=true, to_apply=%region_0.0 | all-reduce | flops 524288 | bytes 3145728 | tf_op jit(solution)/shard_map/psum | solution.py:41
  152.4 0.5 copy.14
  153.0 0.0 all-to-all-done.1
  153.0 1.5 copy.16
  154.5 0.0 all-gather.4.cloned.1.call-done
  154.5 5.6 %convolution_bitcast_fusion.1 = f32[1024,1408]{0,1:T(8,128)} fusion(bf16[512,1408]{1,0:T(8,128)(2,1)} %all-gather.4.cloned.1.call-done, bf16[512,1024]{1,0:T(8,128)(2,1)S(1)} %bitcast.29), kind=kOutput, calls=%fused_computation.2 | convolution fusion | flops 1476395008 | bytes 8257536 | tf_op jit(solution)/shard_map/dot_general | solution.py:8
  160.1 6.2 %copy.17 = f32[1024,1408]{1,0:T(8,128)} copy(f32[1024,1408]{0,1:T(8,128)} %convolution_bitcast_fusion.1) | data formatting | bytes 11534336
  166.3 0.0 all-gather.6.cloned.1.call-done
  166.3 5.6 %convolution_bitcast_fusion = f32[1024,1408]{0,1:T(8,128)} fusion(bf16[512,1408]{1,0:T(8,128)(2,1)} %all-gather.6.cloned.1.call-done, bf16[512,1024]{1,0:T(8,128)(2,1)S(1)} %bitcast.30), kind=kOutput, calls=%fused_computation.1 | convolution fusion | flops 1476395008 | bytes 8257536 | tf_op jit(solution)/shard_map/dot_general | solution.py:8
  171.9 6.2 %copy.18 = f32[1024,1408]{1,0:T(8,128)} copy(f32[1024,1408]{0,1:T(8,128)} %convolution_bitcast_fusion) | data formatting | bytes 11534336
  178.1 0.0 all-gather.8.cloned.1.call-done
  178.1 5.6 %fusion.4 = f32[1408,1024]{1,0:T(8,128)} fusion(bf16[512,1408]{1,0:T(8,128)(2,1)} %all-gather.8.cloned.1.call-done, bf16[512,1024]{1,0:T(8,128)(2,1)S(1)} %bitcast.28), kind=kOutput, calls=%fused_computation.11 | convolution fusion | flops 1476395008 | bytes 8257536 | tf_op jit(solution)/shard_map/dot_general | solution.py:8
Async XLA Ops:
  7.2 8.6 %copy-start.2 = (bf16[128,4096]{1,0:T(8,128)(2,1)S(1)}, bf16[128,4096]{1,0:T(8,128)(2,1)}, u32[]{:S(2)}) copy-start(bf16[128,4096]{1,0:T(8,128)(2,1)} %param.5) | copy-start | bytes 3145732
  7.2 147.3 %all-gather.4.cloned.1.call-start = ((), (), s32[]{:S(2)}) async-start(), calls=%async_computation.2 | async-start | bytes 1802240 | tf_op jit(solution)/shard_map/all_gather | solution.py:34
  7.2 8.6 %copy-start = (bf16[4096,1408]{1,0:T(8,128)(2,1)S(1)}, bf16[4096,1408]{1,0:T(8,128)(2,1)}, u32[]{:S(2)}) copy-start(bf16[4096,1408]{1,0:T(8,128)(2,1)} %param.7) | copy-start | bytes 34603012
  15.8 4.3 %copy-start.1 = (bf16[4096,1408]{1,0:T(8,128)(2,1)S(1)}, bf16[4096,1408]{1,0:T(8,128)(2,1)}, u32[]{:S(2)}) copy-start(bf16[4096,1408]{1,0:T(8,128)(2,1)} %param.8) | copy-start | bytes 34603012
  23.1 9.2 %copy-start.3 = (bf16[128,4096]{1,0:T(8,128)(2,1)S(1)}, bf16[128,4096]{1,0:T(8,128)(2,1)}, u32[]{:S(2)}) copy-start(bf16[128,4096]{1,0:T(8,128)(2,1)} %param.6) | copy-start | bytes 3145732
  23.1 10.5 %copy-start.4 = (bf16[128,1408]{1,0:T(8,128)(2,1)S(1)}, bf16[128,1408]{1,0:T(8,128)(2,1)}, u32[]{:S(2)}) copy-start(bf16[128,1408]{1,0:T(8,128)(2,1)} %get-tuple-element.17) | copy-start | bytes 1081348
  23.1 143.2 %all-gather.6.cloned.1.call-start = ((), (), s32[]{:S(2)}) async-start(), calls=%async_computation.3 | async-start | bytes 1802240 | tf_op jit(solution)/shard_map/all_gather | solution.py:35
  25.2 54.9 %all-to-all-start = ((bf16[128,4,1024]{0,2,1:T(8,128)(2,1)}), bf16[128,4,1024]{0,2,1:T(8,128)(2,1)S(1)}, u32[]{:S(2)}, u32[]{:S(2)}) async-start(bf16[128,4,1024]{0,2,1:T(8,128)(2,1)} %bitcast.27), calls=%async_computation | async-start | bytes 2097152 | tf_op jit(solution)/shard_map/all_to_all | solution.py:31
  31.5 146.6 %all-gather.8.cloned.1.call-start = ((), (), s32[]{:S(2)}) async-start(), calls=%async_computation.4 | async-start | bytes 1802240 | tf_op jit(solution)/shard_map/all_gather | solution.py:36
  80.1 72.9 %all-to-all-start.1 = ((bf16[128,4,1024]{0,2,1:T(8,128)(2,1)}), bf16[128,4,1024]{0,2,1:T(8,128)(2,1)}, u32[]{:S(2)}, u32[]{:S(2)}) async-start(bf16[128,4,1024]{0,2,1:T(8,128)(2,1)} %bitcast.5), calls=%async_computation.1 | async-start | bytes 2097152 | tf_op jit(solution)/shard_map/all_to_all | solution.py:32
Sparse Core Ops, SparseCore 0:
  23.2 57.4 all-gather.3
  82.3 48.3 all-gather.5
  132.3 33.8 all-gather.7
where the time goes:
time: 191 us; the launch traced here: 190 us
  blocking collectives  59.1 us (31%)
  matrix products  48.6 us (25%)
  waiting for transfers between devices  38.5 us (20%)
  local copies, waits for them, and re-layouts  19.5 us (10%)
  between operations  13.9 us (7%)
  starting transfers between devices  10.7 us (6%)
    psum x1, blocking collectives, local(): grad_input = lax.psum(input_terms, ('fs', 'tp')).astype(jnp.bfloat16)  59.1 us
    all_to_all x1, waiting for transfers between devices, local(): lax.all_to_all(inputs, 'rep', split_axis=1, concat_axis=0, tiled=True)  37 us
    dot_general x3, matrix products, contract_cols(): lax.dot_general(left, right, (((1,), (1,)), ((), ())), preferred_element_...  27 us
    unnamed x14, local copies, waits for them, and re-layouts  17.5 us
    dot_general x3, matrix products, contract_rows(): lax.dot_general(left, right, (((0,), (0,)), ((), ())), preferred_element_...  16.7 us
    all_to_all x1, starting transfers between devices, local(): lax.all_to_all(inputs, 'rep', split_axis=1, concat_axis=0, tiled=True)  6.35 us
    all_to_all x1, starting transfers between devices, local(): lax.all_to_all(cotangent, 'rep', split_axis=1, concat_axis=0, tiled=True)  4.27 us
  transfers between devices with their start and end apart: 5, of which 1 were waited for; matrix products, arithmetic and copies ran while one was open for 25% of the time, Pallas kernels for 0%

commit v1 on v0

--- a/solution.py
+++ b/solution.py
@@ -38,7 +38,7 @@
     grad_upward = contract_rows(input_cols, piece_up)
     grad_down = contract_rows(piece_hidden, cotangent_cols)
     input_terms = contract_cols(gate_delta, w_gate) + contract_cols(up_delta, w_upward)
-    grad_input = lax.psum(input_terms, ("fs", "tp")).astype(jnp.bfloat16)
+    grad_input = jnp.sum(lax.all_gather(input_terms, ("fs", "tp")), axis=0).astype(jnp.bfloat16)
     return (grad_input, grad_gate, grad_upward, grad_down)
 
 

time: 191 us -> 265 us (1.39)
  waiting for transfers between devices: 38.5 us -> 165 us
  blocking collectives: 59.1 us -> 0 us
  other arithmetic: 0 us -> 8.43 us
    all_gather x0 -> x1, waiting for transfers between devices: none -> 84.9 us  [local(): lax.all_gather(input_terms, ('fs', 'tp'))]
    psum x1 -> x0, blocking collectives: 59.1 us -> none  [local(): grad_input = lax.psum(input_terms, ('fs', 'tp')).astype(jnp.bfloat16)]
    all_to_all x1, waiting for transfers between devices: 0.01 us -> 35.6 us  [local(): lax.all_to_all(cotangent, 'rep', split_axis=1, concat_axis=0, tiled=True)]
    reduce_sum x0 -> x1, other arithmetic: none -> 8.43 us  [local(): jnp.sum(lax.all_gather(input_terms, ('fs', 'tp')), axis=0)]
    all_gather x1, waiting for transfers between devices: 0.01 us -> 5.83 us  [local(): piece_hidden = lax.all_gather(hidden, 'rep', axis=0, tiled=True)]
  transfers between devices with their start and end apart: 5 -> 6, of which waited for: 1 -> 4; matrix products, arithmetic and copies ran while one was open for 25% -> 19% of each run, Pallas kernels for 0% -> 0%
where the time goes in v1:
time: 265 us; the launch traced here: 264 us
  waiting for transfers between devices  165 us (62%)
  matrix products  48 us (18%)
  local copies, waits for them, and re-layouts  18.6 us (7%)
  between operations  13.9 us (5%)
  starting transfers between devices  10 us (4%)
  other arithmetic  8.43 us (3%)
    all_gather x1, waiting for transfers between devices, local(): lax.all_gather(input_terms, ('fs', 'tp'))  84.9 us
    all_to_all x1, waiting for transfers between devices, local(): lax.all_to_all(inputs, 'rep', split_axis=1, concat_axis=0, tiled=True)  37.5 us
    all_to_all x1, waiting for transfers between devices, local(): lax.all_to_all(cotangent, 'rep', split_axis=1, concat_axis=0, tiled=True)  35.6 us
    dot_general x3, matrix products, contract_cols(): lax.dot_general(left, right, (((1,), (1,)), ((), ())), preferred_element_...  26.4 us
    unnamed x14, local copies, waits for them, and re-layouts  17.5 us
    dot_general x3, matrix products, contract_rows(): lax.dot_general(left, right, (((0,), (0,)), ((), ())), preferred_element_...  16.8 us
    reduce_sum x1, other arithmetic, local(): jnp.sum(lax.all_gather(input_terms, ('fs', 'tp')), axis=0)  8.43 us
    all_to_all x1, starting transfers between devices, local(): lax.all_to_all(inputs, 'rep', split_axis=1, concat_axis=0, tiled=True)  6.19 us
  transfers between devices with their start and end apart: 6, of which 4 were waited for; matrix products, arithmetic and copies ran while one was open for 19% of the time, Pallas kernels for 0%

profile of v1, /device:TPU:0, one launch (start us, length us, event | category | flops | bytes accessed | tf_op | source)
XLA Modules:
  0.0 264.2 jit_solution(18267900097118225035)
XLA Ops:
  7.2 0.0 copy-start.2
  7.2 0.0 all-gather.6.cloned.1.call-start
  7.2 0.0 copy-start
  7.2 8.6 %fusion.1 = f32[128,1408]{1,0:T(8,128)S(1)} fusion(bf16[128,4096]{1,0:T(8,128)(2,1)} %param.6, bf16[1408,4096]{1,0:T(8,128)(2,1)} %param.9), kind=kOutput, calls=%fused_computation.8 | convolution fusion | flops 1476395008 | bytes 13303808 | tf_op jit(solution)/shard_map/dot_general | solution.py:14
  15.8 0.0 copy-done.2
  15.8 0.0 copy-done
  15.8 0.0 copy-start.1
  15.8 1.8 fusion.2
  17.7 2.4 copy-done.1
  20.1 3.0 %multiply_convert_fusion = (bf16[128,1408]{1,0:T(8,128)(2,1)}, bf16[128,1408]{1,0:T(8,128)(2,1)}, bf16[128,1408]{1,0:T(8,128)(2,1)}) fusion(f32[128,1408]{1,0:T(8,128)S(1)} %fusion.2, f32[128,1408]{1,0:T(8,128)S(1)} %fusion.1, bf16[128,4096]{1,0:T(8,128)(2,1)S(1)} %copy-done.2, bf16[4096,1408]{1,0:T(8,128)(2,1)S(1)} %copy-done.1), kind=kOutput, calls=%fused_computation.3 | convolution fusion | flops 1479098368 | bytes 15106048 | tf_op jit(solution)/shard_map/dot_general | solution.py:21
  23.1 0.0 all-gather.6.cloned.1.call-update
  23.1 0.0 all-gather.8.cloned.1.call-start
  23.2 0.7 all-gather.8.cloned.1.call-update
  23.9 0.0 all-gather.10.cloned.1.call-start
  23.9 0.7 all-gather.10.cloned.1.call-update
  24.6 0.0 copy-start.4
  24.6 0.0 all-gather.12.cloned.1.call-start
  24.7 8.2 %fusion.3 = f32[128,4096]{1,0:T(8,128)S(1)} fusion(bf16[128,1408]{1,0:T(8,128)(2,1)} %get-tuple-element.17, bf16[4096,1408]{1,0:T(8,128)(2,1)} %param.7), kind=kOutput, calls=%fused_computation.10 | convolution fusion | flops 1476395008 | bytes 13991936 | tf_op jit(solution)/shard_map/dot_general | solution.py:14
  32.9 0.0 copy-done.4
  32.9 9.6 %convolution_add_fusion = f32[128,4096]{1,0:T(8,128)} fusion(f32[128,4096]{1,0:T(8,128)S(1)} %fusion.3, bf16[128,1408]{1,0:T(8,128)(2,1)S(1)} %copy-done.4, bf16[4096,1408]{1,0:T(8,128)(2,1)} %param.8), kind=kOutput, calls=%fused_computation | convolution fusion | flops 1476919296 | bytes 16089088 | tf_op jit(solution)/shard_map/dot_general | solution.py:14
  42.5 0.0 copy-start.3
  42.5 0.0 all-gather.12.cloned.1.call-update
  42.5 1.3 copy.13
  43.8 6.2 %all-to-all-start = ((bf16[128,4,1024]{0,2,1:T(8,128)(2,1)}), bf16[128,4,1024]{0,2,1:T(8,128)(2,1)S(1)}, u32[]{:S(2)}, u32[]{:S(2)}) async-start(bf16[128,4,1024]{0,2,1:T(8,128)(2,1)} %bitcast.1), calls=%async_computation | async-start | bytes 2097152 | tf_op jit(solution)/shard_map/all_to_all | solution.py:31
  50.0 0.0 copy-done.3
  50.0 1.3 copy.15
  51.3 37.5 %all-to-all-done = bf16[128,4,1024]{0,2,1:T(8,128)(2,1)S(1)} async-done(((bf16[128,4,1024]{0,2,1:T(8,128)(2,1)}), bf16[128,4,1024]{0,2,1:T(8,128)(2,1)S(1)}, u32[]{:S(2)}, u32[]{:S(2)}) %all-to-all-start) | async-done | bytes 1048608 | tf_op jit(solution)/shard_map/all_to_all | solution.py:31
  88.8 3.7 %all-to-all-start.1 = ((bf16[128,4,1024]{0,2,1:T(8,128)(2,1)}), bf16[128,4,1024]{0,2,1:T(8,128)(2,1)S(1)}, u32[]{:S(2)}, u32[]{:S(2)}) async-start(bf16[128,4,1024]{0,2,1:T(8,128)(2,1)} %bitcast.6), calls=%async_computation.1 | async-start | bytes 2097152 | tf_op jit(solution)/shard_map/all_to_all | solution.py:32
  92.5 0.5 copy.14
  93.1 35.6 %all-to-all-done.1 = bf16[128,4,1024]{0,2,1:T(8,128)(2,1)S(1)} async-done(((bf16[128,4,1024]{0,2,1:T(8,128)(2,1)}), bf16[128,4,1024]{0,2,1:T(8,128)(2,1)S(1)}, u32[]{:S(2)}, u32[]{:S(2)}) %all-to-all-start.1) | async-done | bytes 1048608 | tf_op jit(solution)/shard_map/all_to_all | solution.py:32
  128.7 0.5 copy.16
  129.2 0.0 all-gather.6.cloned.1.call-done
  129.3 5.6 %convolution_bitcast_fusion.1 = f32[1024,1408]{0,1:T(8,128)} fusion(bf16[512,1408]{1,0:T(8,128)(2,1)} %all-gather.6.cloned.1.call-done, bf16[512,1024]{1,0:T(8,128)(2,1)S(1)} %bitcast.31), kind=kOutput, calls=%fused_computation.2 | convolution fusion | flops 1476395008 | bytes 8257536 | tf_op jit(solution)/shard_map/dot_general | solution.py:8
  134.9 6.2 %copy.17 = f32[1024,1408]{1,0:T(8,128)} copy(f32[1024,1408]{0,1:T(8,128)} %convolution_bitcast_fusion.1) | data formatting | bytes 11534336
  141.1 0.0 all-gather.8.cloned.1.call-done
  141.1 5.6 %convolution_bitcast_fusion = f32[1024,1408]{0,1:T(8,128)} fusion(bf16[512,1408]{1,0:T(8,128)(2,1)} %all-gather.8.cloned.1.call-done, bf16[512,1024]{1,0:T(8,128)(2,1)S(1)} %bitcast.32), kind=kOutput, calls=%fused_computation.1 | convolution fusion | flops 1476395008 | bytes 8257536 | tf_op jit(solution)/shard_map/dot_general | solution.py:8
  146.7 6.2 %copy.18 = f32[1024,1408]{1,0:T(8,128)} copy(f32[1024,1408]{0,1:T(8,128)} %convolution_bitcast_fusion) | data formatting | bytes 11534336
  152.9 5.8 %all-gather.10.cloned.1.call-done = bf16[512,1408]{1,0:T(8,128)(2,1)} async-done(((bf16[128,1408]{1,0:T(8,128)(2,1)}), bf16[512,1408]{1,0:T(8,128)(2,1)}) %all-gather.10.cloned.1.call-update) | async-done | bytes 1441808 | tf_op jit(solution)/shard_map/all_gather | solution.py:36
  158.8 5.6 %fusion.4 = f32[1408,1024]{1,0:T(8,128)} fusion(bf16[512,1408]{1,0:T(8,128)(2,1)} %all-gather.10.cloned.1.call-done, bf16[512,1024]{1,0:T(8,128)(2,1)S(1)} %bitcast.30), kind=kOutput, calls=%fused_computation.11 | convolution fusion | flops 1476395008 | bytes 8257536 | tf_op jit(solution)/shard_map/dot_general | solution.py:8
  164.3 84.9 %all-gather.12.cloned.1.call-done = f32[1024,4096]{1,0:T(8,128)} async-done(((f32[128,4096]{1,0:T(8,128)}), f32[1024,4096]{1,0:T(8,128)}) %all-gather.12.cloned.1.call-update) | async-done | bytes 16777232 | tf_op jit(solution)/shard_map/all_gather | solution.py:41
  249.2 8.4 %reduce_sum.9 = bf16[128,4096]{1,0:T(8,128)(2,1)} reduce(f32[8,128,4096]{2,1,0:T(8,128)} %bitcast.27, f32[]{:T(128)} %constant.1.clone.1), dimensions={0}, to_apply=%region_0.0 | reduce | flops 3670016 | bytes 17825796 | tf_op jit(solution)/shard_map/reduce_sum | solution.py:41
Async XLA Ops:
  7.2 8.6 %copy-start.2 = (bf16[128,4096]{1,0:T(8,128)(2,1)S(1)}, bf16[128,4096]{1,0:T(8,128)(2,1)}, u32[]{:S(2)}) copy-start(bf16[128,4096]{1,0:T(8,128)(2,1)} %param.5) | copy-start | bytes 3145732
  7.2 122.1 %all-gather.6.cloned.1.call-start = ((), (), s32[]{:S(2)}) async-start(), calls=%async_computation.2 | async-start | bytes 1802240 | tf_op jit(solution)/shard_map/all_gather | solution.py:34
  7.2 8.6 %copy-start = (bf16[4096,1408]{1,0:T(8,128)(2,1)S(1)}, bf16[4096,1408]{1,0:T(8,128)(2,1)}, u32[]{:S(2)}) copy-start(bf16[4096,1408]{1,0:T(8,128)(2,1)} %param.7) | copy-start | bytes 34603012
  15.8 4.3 %copy-start.1 = (bf16[4096,1408]{1,0:T(8,128)(2,1)S(1)}, bf16[4096,1408]{1,0:T(8,128)(2,1)}, u32[]{:S(2)}) copy-start(bf16[4096,1408]{1,0:T(8,128)(2,1)} %param.8) | copy-start | bytes 34603012
  23.1 118.0 %all-gather.8.cloned.1.call-start = ((), (), s32[]{:S(2)}) async-start(), calls=%async_computation.3 | async-start | bytes 1802240 | tf_op jit(solution)/shard_map/all_gather | solution.py:35
  23.9 134.9 %all-gather.10.cloned.1.call-start = ((), (), s32[]{:S(2)}) async-start(), calls=%async_computation.4 | async-start | bytes 1802240 | tf_op jit(solution)/shard_map/all_gather | solution.py:36
  24.6 8.3 %copy-start.4 = (bf16[128,1408]{1,0:T(8,128)(2,1)S(1)}, bf16[128,1408]{1,0:T(8,128)(2,1)}, u32[]{:S(2)}) copy-start(bf16[128,1408]{1,0:T(8,128)(2,1)} %get-tuple-element.18) | copy-start | bytes 1081348
  24.6 224.6 %all-gather.12.cloned.1.call-start = ((), (), s32[]{:S(2)}) async-start(), calls=%async_computation.5 | async-start | bytes 18874368 | tf_op jit(solution)/shard_map/all_gather | solution.py:41
  42.5 7.5 %copy-start.3 = (bf16[128,4096]{1,0:T(8,128)(2,1)S(1)}, bf16[128,4096]{1,0:T(8,128)(2,1)}, u32[]{:S(2)}) copy-start(bf16[128,4096]{1,0:T(8,128)(2,1)} %param.6) | copy-start | bytes 3145732
  43.8 45.0 %all-to-all-start = ((bf16[128,4,1024]{0,2,1:T(8,128)(2,1)}), bf16[128,4,1024]{0,2,1:T(8,128)(2,1)S(1)}, u32[]{:S(2)}, u32[]{:S(2)}) async-start(bf16[128,4,1024]{0,2,1:T(8,128)(2,1)} %bitcast.1), calls=%async_computation | async-start | bytes 2097152 | tf_op jit(solution)/shard_map/all_to_all | solution.py:31
  88.8 39.9 %all-to-all-start.1 = ((bf16[128,4,1024]{0,2,1:T(8,128)(2,1)}), bf16[128,4,1024]{0,2,1:T(8,128)(2,1)S(1)}, u32[]{:S(2)}, u32[]{:S(2)}) async-start(bf16[128,4,1024]{0,2,1:T(8,128)(2,1)} %bitcast.6), calls=%async_computation.1 | async-start | bytes 2097152 | tf_op jit(solution)/shard_map/all_to_all | solution.py:32
Sparse Core Ops, SparseCore 0:
  23.3 46.7 all-gather.5
  71.6 52.1 all-gather.7
  125.4 33.3 all-gather.9
  160.5 88.7 all-gather.11
